TPU v7x, 32 devices: a whole 2x2x4 slice. The times are simulated.
32 devices in a mesh: fs: 8 (over z, y), tp: 4 (over x, core).
Axes of the slice: x: 2, y: 2, z: 4, core: 2. Of those that a mesh axis runs over, the one named last changes fastest.
Arguments:
- tokens: bfloat16 [4096, 2048], P('fs', 'tp'), may hold values from -6 to 6
- mixer_gain: float32 [2048], replicated, may hold values from 0.1 to 1.9
- recur_in: bfloat16 [2048, 1024], P('fs', 'tp'), may hold values from -0.125 to 0.125
- branch_in: bfloat16 [2048, 1024], P('fs', 'tp'), may hold values from -0.125 to 0.125
- conv_taps: bfloat16 [4, 1024], replicated, may hold values from -3 to 3
- recur_gate: bfloat16 [2, 16, 64, 64], replicated, may hold values from -0.75 to 0.75
- input_gate: bfloat16 [2, 16, 64, 64], replicated, may hold values from -0.75 to 0.75
- decay_param: float32 [2, 1024], replicated, may hold values from 3.5 to 11
- recur_gain: float32 [1024], replicated, may hold values from 0.1 to 1.9
- recur_out: bfloat16 [1024, 2048], P('tp', 'fs'), may hold values from -0.1875 to 0.1875
- mixer_post: float32 [2048], replicated, may hold values from 0.1 to 1.9
- channel_gain: float32 [2048], replicated, may hold values from 0.1 to 1.9
- hidden_gate: bfloat16 [2048, 5632], P('fs', 'tp'), may hold values from -0.125 to 0.125
- hidden_up: bfloat16 [2048, 5632], P('fs', 'tp'), may hold values from -0.125 to 0.125
- hidden_down: bfloat16 [5632, 2048], P('tp', 'fs'), may hold values from -0.078125 to 0.078125
- channel_post: float32 [2048], replicated, may hold values from 0.1 to 1.9
Outputs:
- layer_out: bfloat16 [4096, 2048], P('fs', 'tp')
All inputs are finite; a program needn't handle non-finite values.
Results may differ from a plain program's by a relative error of at most 0.018.
Values may be sent and summed in bfloat16 or wider, within the bound.
A program may use at most 64 MiB of HBM per device.

v0:
```python
import jax
import jax.numpy as jnp
from jax import lax
from jax.sharding import PartitionSpec as P

D = 2048
BLOCK = 64
EPS = 1e-06
SHRINK = 8.0


def rms_scale(values, gain):
    return values * lax.rsqrt(jnp.mean(values * values, axis=-1, keepdims=True) + EPS) * gain


def linear_scan(decay, inflow, reverse):

    def combine(former, latter):
        return (former[0] * latter[0], latter[0] * former[1] + latter[1])

    return lax.associative_scan(combine, (decay, inflow), axis=0, reverse=reverse)[1]


def short_conv(recur_x, taps):
    length = recur_x.shape[0]
    padded = jnp.pad(recur_x.astype(jnp.float32), ((2, 1), (0, 0)))
    total = taps[0] * padded[0:length]
    for position in range(1, taps.shape[0]):
        total = total + taps[position] * padded[position : position + length]
    return total


def recurrence(conv_out, rate_weight, inlet_weight, decay_row, reverse):
    length, width = conv_out.shape
    grouped = conv_out.reshape(length, rate_weight.shape[0], rate_weight.shape[1])
    rate = jax.nn.sigmoid(
        jnp.einsum(
            "lhi,hij->lhj",
            grouped,
            rate_weight.astype(jnp.float32),
            precision=lax.Precision.HIGHEST,
        ).reshape(length, width)
    )
    inlet = jax.nn.sigmoid(
        jnp.einsum(
            "lhi,hij->lhj",
            grouped,
            inlet_weight.astype(jnp.float32),
            precision=lax.Precision.HIGHEST,
        ).reshape(length, width)
    )
    log_decay = -SHRINK * rate * jax.nn.softplus(-decay_row)
    inflow = conv_out * inlet * jnp.sqrt(-jnp.expm1(2.0 * log_decay))
    return linear_scan(jnp.exp(log_decay), inflow, reverse)


def add_slab(source, piece):
    return jnp.dot(source, piece, preferred_element_type=jnp.float32)


def on_device(
    tokens,
    mixer_gain,
    recur_in,
    branch_in,
    conv_taps,
    recur_gate,
    input_gate,
    decay_param,
    recur_gain,
    recur_out,
    mixer_post,
    channel_gain,
    hidden_gate,
    hidden_up,
    hidden_down,
    channel_post,
):
    rank_tp = lax.axis_index("tp")
    feature_width = tokens.shape[1]
    channel_width = recur_in.shape[1]
    group_count = channel_width // BLOCK
    feature_start = rank_tp * feature_width
    channel_start = rank_tp * channel_width
    gathered_in = lax.all_gather(tokens, "tp", axis=1, tiled=True)
    gathered_float = gathered_in.astype(jnp.float32)
    normed_in = rms_scale(gathered_float, mixer_gain).astype(jnp.bfloat16)

    def add_mixer(piece):
        return add_slab(normed_in, piece)

    recur_total = add_mixer(lax.all_gather(recur_in, "fs", axis=0, tiled=True))
    branch_total = add_mixer(lax.all_gather(branch_in, "fs", axis=0, tiled=True))
    recur_x = recur_total.astype(jnp.bfloat16)
    branch_x = branch_total.astype(jnp.bfloat16)
    taps = lax.dynamic_slice_in_dim(conv_taps, channel_start, channel_width, 1).astype(jnp.float32)
    conv_out = short_conv(recur_x, taps)
    group_start = rank_tp * group_count
    rate_own = lax.dynamic_slice_in_dim(recur_gate, group_start, group_count, 1)
    inlet_own = lax.dynamic_slice_in_dim(input_gate, group_start, group_count, 1)
    decay_own = lax.dynamic_slice_in_dim(decay_param, channel_start, channel_width, 1)
    forward = recurrence(conv_out, rate_own[0], inlet_own[0], decay_own[0], False)
    backward = recurrence(conv_out, rate_own[1], inlet_own[1], decay_own[1], True)
    mixed = (forward + backward) * jax.nn.gelu(branch_x.astype(jnp.float32))
    gain_own = lax.dynamic_slice_in_dim(recur_gain, channel_start, channel_width, 0)
    recur_y = (mixed * gain_own).astype(jnp.bfloat16)
    branch_part = jnp.dot(
        recur_y,
        lax.all_gather(recur_out, "fs", axis=1, tiled=True),
        preferred_element_type=jnp.float32,
    )
    branch_sum = lax.psum(branch_part.astype(jnp.bfloat16), "tp").astype(jnp.float32)
    mid_full = (gathered_float + rms_scale(branch_sum, mixer_post)).astype(jnp.bfloat16)
    mid_own = lax.dynamic_slice_in_dim(mid_full, feature_start, feature_width, 1)
    channel_in = rms_scale(mid_full.astype(jnp.float32), channel_gain).astype(jnp.bfloat16)

    def add_channel(piece):
        return add_slab(channel_in, piece)

    gate_total = add_channel(lax.all_gather(hidden_gate, "fs", axis=0, tiled=True))
    up_total = add_channel(lax.all_gather(hidden_up, "fs", axis=0, tiled=True))
    hidden = (jax.nn.silu(gate_total) * up_total).astype(jnp.bfloat16)
    hidden_part = jnp.dot(
        hidden,
        lax.all_gather(hidden_down, "fs", axis=1, tiled=True),
        preferred_element_type=jnp.float32,
    )
    hidden_own = lax.psum_scatter(
        hidden_part.astype(jnp.bfloat16), "tp", scatter_dimension=1, tiled=True
    ).astype(jnp.float32)
    hidden_energy = lax.psum(jnp.sum(hidden_own * hidden_own, axis=1), "tp")
    close_own = lax.dynamic_slice_in_dim(channel_post, feature_start, feature_width, 0)
    return (
        mid_own.astype(jnp.float32)
        + hidden_own * lax.rsqrt(hidden_energy / D + EPS)[:, None] * close_own
    ).astype(jnp.bfloat16)


def solution(mesh):
    in_specs = (
        P("fs", "tp"),
        P(),
        P("fs", "tp"),
        P("fs", "tp"),
        P(),
        P(),
        P(),
        P(),
        P(),
        P("tp", "fs"),
        P(),
        P(),
        P("fs", "tp"),
        P("fs", "tp"),
        P("tp", "fs"),
        P(),
    )
    out_specs = P("fs", "tp")
    return jax.shard_map(
        on_device, mesh=mesh, in_specs=in_specs, out_specs=out_specs, check_vma=False
    )
```

profile of v0, /device:TPU:0, one launch (start us, length us, event | category | flops | bytes accessed | tf_op | source)
XLA Modules:
  0.0 592.1 jit_solution(11456441102849634958)
XLA Ops:
  10.1 1.3 dynamic_slice.25
  12.3 21.9 %all-gather.8.cloned.1.call-done = bf16[512,2048]{1,0:T(8,128)(2,1)} async-done(((bf16[512,512]{1,0:T(8,128)(2,1)}), bf16[512,2048]{1,0:T(8,128)(2,1)}) %all-gather.8.cloned.1.call-update) | async-done | bytes 2097168 | tf_op jit(solution)/shard_map/all_gather | solution.py:85
  34.2 2.1 fusion.5
  36.3 40.3 %all-gather.10.cloned.1.call-done = bf16[2048,256]{1,0:T(8,128)(2,1)} async-done(((bf16[256,256]{1,0:T(8,128)(2,1)}), bf16[2048,256]{1,0:T(8,128)(2,1)}) %all-gather.10.cloned.1.call-update) | async-done | bytes 1048592 | tf_op jit(solution)/shard_map/all_gather | solution.py:92
  76.6 2.6 fusion.22
  80.7 2.1 fusion.21
  82.9 1.3 fusion.17
  85.2 2.0 copy.33
  89.2 2.5 multiply_exponential_fusion
  92.3 1.4 slice.487
  93.7 1.4 slice.485
  95.0 1.4 slice.489
  96.4 1.2 fusion.95
  99.8 1.1 fusion.97
  106.9 1.4 fusion.101
  108.4 1.4 slice.510
  109.7 1.4 slice.511
  111.1 1.4 slice.509
  112.4 1.4 slice.513
  113.8 1.4 fusion.103
  116.4 1.3 slice.515
  117.7 1.3 slice.519
  119.0 1.3 fusion.105
  120.3 1.3 slice.522
  121.6 1.3 slice.523
  122.9 1.3 slice.521
  124.2 1.3 slice.525
  125.5 1.3 fusion.108
  126.8 1.3 slice.528
  128.1 1.3 slice.529
  129.3 1.3 slice.527
  130.6 1.3 slice.531
  133.3 1.3 fusion.107
  135.2 1.3 slice.520
  136.5 1.3 slice.537
  137.8 1.3 slice.636
  139.0 1.3 slice.514
  142.3 1.4 slice.541
  143.7 1.3 slice.634
  153.2 1.3 slice.561
  154.7 1.0 fusion.96
  165.9 1.4 slice.554
  167.3 1.4 slice.624
  179.0 1.7 pad.132
  181.4 1.7 pad.131
  183.9 1.7 pad.150
  185.6 1.8 slice.555
  187.4 3.0 slice.625
  190.5 1.0 fusion.57
  191.6 1.9 add.409
  193.5 3.4 rev.2
  197.0 5.7 convolution_convert_fusion
  205.1 47.9 %all-reduce.39.cloned.1.call-done = bf16[512,2048]{1,0:T(8,128)(2,1)} async-done(((bf16[512,2048]{1,0:T(8,128)(2,1)}), bf16[512,2048]{1,0:T(8,128)(2,1)}) %all-reduce.39.cloned.1.call-update) | async-done | bytes 2097168 | tf_op jit(solution)/shard_map/psum | solution.py:112
  253.0 2.1 fusion
  255.1 4.0 fusion.2
  259.2 88.3 %all-gather.16.cloned.1.call-done = bf16[2048,1408]{1,0:T(8,128)(2,1)} async-done(((bf16[256,1408]{1,0:T(8,128)(2,1)}), bf16[2048,1408]{1,0:T(8,128)(2,1)}) %all-gather.16.cloned.1.call-update) | async-done | bytes 5767184 | tf_op jit(solution)/shard_map/all_gather | solution.py:120
  347.5 8.5 %fusion.30 = f32[512,1408]{1,0:T(8,128)} fusion(bf16[2048,1408]{1,0:T(8,128)(2,1)} %all-gather.16.cloned.1.call-done, bf16[512,2048]{1,0:T(8,128)(2,1)} %get-tuple-element.6, f32[2048]{0:T(1024)S(1)} %copy-done.23, f32[512]{0:T(512)S(1)} %add_rsqrt_fusion.1), kind=kOutput, calls=%fused_computation.47 | convolution fusion | flops 2956984320 | bytes 10758144 | tf_op jit(solution)/shard_map/dot_general | solution.py:58
  356.0 84.2 %all-gather.18.cloned.1.call-done = bf16[2048,1408]{1,0:T(8,128)(2,1)} async-done(((bf16[256,1408]{1,0:T(8,128)(2,1)}), bf16[2048,1408]{1,0:T(8,128)(2,1)}) %all-gather.18.cloned.1.call-update) | async-done | bytes 5767184 | tf_op jit(solution)/shard_map/all_gather | solution.py:121
  440.2 93.4 %all-gather.20.cloned.1.call-done = bf16[1408,2048]{1,0:T(8,128)(2,1)} async-done(((bf16[1408,256]{1,0:T(8,128)(2,1)}), bf16[1408,2048]{1,0:T(8,128)(2,1)}) %all-gather.20.cloned.1.call-update) | async-done | bytes 5767184 | tf_op jit(solution)/shard_map/all_gather | solution.py:125
  533.6 13.4 %convolution_convert_fusion.1 = bf16[512,2048]{1,0:T(8,128)(2,1)} fusion(bf16[1408,2048]{1,0:T(8,128)(2,1)} %all-gather.20.cloned.1.call-done, bf16[2048,1408]{1,0:T(8,128)(2,1)} %all-gather.18.cloned.1.call-done, f32[512,1408]{1,0:T(8,128)} %fusion.30, bf16[512,2048]{1,0:T(8,128)(2,1)S(1)} %copy-done.2, f32[2048]{0:T(1024)S(1)} %copy-done.23, ...), kind=kOutput, calls=%fused_computation.19 | convolution fusion | flops 5915148288 | bytes 18622464 | tf_op jit(solution)/shard_map/dot_general | solution.py:123
  547.7 28.7 %reduce-scatter.2.cloned.1.call-done = bf16[512,512]{1,0:T(8,128)(2,1)} async-done(((bf16[512,2048]{1,0:T(8,128)(2,1)}), bf16[512,512]{1,0:T(8,128)(2,1)}) %reduce-scatter.2.cloned.1.call-update) | async-done | bytes 524304 | tf_op jit(solution)/shard_map/reduce_scatter | solution.py:128
  576.5 1.2 fusion.24
  577.7 5.8 psum.15
  583.5 2.1 fusion.27
  (253 shorter events, 55.7 us)
Async XLA Ops:
  6.5 73.2 %copy-start = (bf16[2,16,64,64]{3,2,1,0:T(8,128)(2,1)S(1)}, bf16[2,16,64,64]{3,2,1,0:T(8,128)(2,1)}, u32[]{:S(2)}) copy-start(bf16[2,16,64,64]{3,2,1,0:T(8,128)(2,1)} %param.22) | copy-start | bytes 786436
  6.5 27.7 %all-gather.8.cloned.1.call-start = ((), (), s32[]{:S(2)}) async-start(), calls=%async_computation.1 | async-start | bytes 2621440 | tf_op jit(solution)/shard_map/all_gather | solution.py:85
  7.3 69.4 %all-gather.10.cloned.1.call-start = ((), (), s32[]{:S(2)}) async-start(), calls=%async_computation.2 | async-start | bytes 1179648 | tf_op jit(solution)/shard_map/all_gather | solution.py:92
  8.0 189.0 %all-gather.12.cloned.1.call-start = ((), (), s32[]{:S(2)}) async-start(), calls=%async_computation.3 | async-start | bytes 1179648 | tf_op jit(solution)/shard_map/all_gather | solution.py:93
  8.7 188.2 %all-gather.14.cloned.1.call-start = ((), (), s32[]{:S(2)}) async-start(), calls=%async_computation.4 | async-start | bytes 1179648 | tf_op jit(solution)/shard_map/all_gather | solution.py:109
  9.3 243.7 %all-reduce.39.cloned.1.call-start = ((), (), s32[]{:S(2)}) async-start(), calls=%async_computation.5 | async-start | bytes 4194304 | tf_op jit(solution)/shard_map/psum | solution.py:112
  36.3 43.0 %copy-start.19 = (f32[512]{0:T(512)}, f32[512]{0:T(512)S(1)}, u32[]{:S(2)}) copy-start(f32[512]{0:T(512)S(1)} %add_rsqrt_fusion.3) | copy-start | bytes 6148
  155.7 22.4 %copy-start.3 = (f32[127,256]{1,0:T(8,128)S(1)}, f32[127,256]{1,0:T(8,128)}, u32[]{:S(2)}) copy-start(f32[127,256]{1,0:T(8,128)} %slice.547) | copy-start | bytes 390148
  168.7 14.4 %copy-start.17 = (f32[1,256]{1,0:T(1,128)S(1)}, f32[1,256]{1,0:T(1,128)}, u32[]{:S(2)}) copy-start(f32[1,256]{1,0:T(1,128)} %get-tuple-element.41) | copy-start | bytes 3076
  168.7 14.4 %copy-start.18 = (f32[1,256]{1,0:T(1,128)S(1)}, f32[1,256]{1,0:T(1,128)}, u32[]{:S(2)}) copy-start(f32[1,256]{1,0:T(1,128)} %get-tuple-element.42) | copy-start | bytes 3076
  168.7 14.4 %copy-start.9 = (f32[2,256]{1,0:T(2,128)S(1)}, f32[2,256]{1,0:T(2,128)}, u32[]{:S(2)}) copy-start(f32[2,256]{1,0:T(2,128)} %pad_add_fusion) | copy-start | bytes 6148
  170.0 13.2 %copy-start.6 = (f32[3,256]{1,0:T(4,128)S(1)}, f32[3,256]{1,0:T(4,128)}, u32[]{:S(2)}) copy-start(f32[3,256]{1,0:T(4,128)} %slice.595) | copy-start | bytes 9220
  170.0 13.2 %copy-start.7 = (f32[3,256]{1,0:T(4,128)S(1)}, f32[3,256]{1,0:T(4,128)}, u32[]{:S(2)}) copy-start(f32[3,256]{1,0:T(4,128)} %slice.612) | copy-start | bytes 9220
  170.7 12.6 %copy-start.16 = (f32[1,256]{1,0:T(1,128)S(1)}, f32[1,256]{1,0:T(1,128)}, u32[]{:S(2)}) copy-start(f32[1,256]{1,0:T(1,128)} %slice.666) | copy-start | bytes 3076
  172.0 11.2 %copy-start.4 = (f32[7,256]{1,0:T(8,128)S(1)}, f32[7,256]{1,0:T(8,128)}, u32[]{:S(2)}) copy-start(f32[7,256]{1,0:T(8,128)} %slice.589) | copy-start | bytes 21508
  172.0 11.2 %copy-start.5 = (f32[7,256]{1,0:T(8,128)S(1)}, f32[7,256]{1,0:T(8,128)}, u32[]{:S(2)}) copy-start(f32[7,256]{1,0:T(8,128)} %slice.614) | copy-start | bytes 21508
  172.1 11.2 %copy-start.15 = (f32[1,256]{1,0:T(1,128)S(1)}, f32[1,256]{1,0:T(1,128)}, u32[]{:S(2)}) copy-start(f32[1,256]{1,0:T(1,128)} %slice.665) | copy-start | bytes 3076
  174.2 9.2 %copy-start.14 = (f32[1,256]{1,0:T(1,128)S(1)}, f32[1,256]{1,0:T(1,128)}, u32[]{:S(2)}) copy-start(f32[1,256]{1,0:T(1,128)} %slice.664) | copy-start | bytes 3076
  175.7 7.8 %copy-start.13 = (f32[1,256]{1,0:T(1,128)S(1)}, f32[1,256]{1,0:T(1,128)}, u32[]{:S(2)}) copy-start(f32[1,256]{1,0:T(1,128)} %slice.663) | copy-start | bytes 3076
  177.4 6.2 %copy-start.12 = (f32[1,256]{1,0:T(1,128)S(1)}, f32[1,256]{1,0:T(1,128)}, u32[]{:S(2)}) copy-start(f32[1,256]{1,0:T(1,128)} %slice.662) | copy-start | bytes 3076
  178.2 5.6 copy-start.11
  183.1 8.4 %copy-start.10 = (f32[1,256]{1,0:T(1,128)S(1)}, f32[1,256]{1,0:T(1,128)}, u32[]{:S(2)}) copy-start(f32[1,256]{1,0:T(1,128)} %slice.660) | copy-start | bytes 3076
  183.8 13.2 %copy-start.1 = (bf16[512,2048]{1,0:T(8,128)(2,1)S(1)}, bf16[512,2048]{1,0:T(8,128)(2,1)}, u32[]{:S(2)}) copy-start(bf16[512,2048]{1,0:T(8,128)(2,1)} %all-gather.8.cloned.1.call-done) | copy-start | bytes 6291460
  183.8 13.2 %copy-start.20 = (f32[512]{0:T(512)S(1)}, f32[512]{0:T(512)}, u32[]{:S(2)}) copy-start(f32[512]{0:T(512)} %copy-done.19) | copy-start | bytes 6148
  183.8 13.2 %copy-start.21 = (f32[256]{0:T(256)S(1)}, f32[256]{0:T(256)}, u32[]{:S(2)}) copy-start(f32[256]{0:T(256)} %dynamic_slice.25) | copy-start | bytes 3076
  183.8 13.2 %copy-start.22 = (f32[2048]{0:T(1024)S(1)}, f32[2048]{0:T(1024)}, u32[]{:S(2)}) copy-start(f32[2048]{0:T(1024)} %param.17) | copy-start | bytes 24580
  202.7 52.4 %copy-start.8 = (f32[2048]{0:T(1024)S(1)}, f32[2048]{0:T(1024)}, u32[]{:S(2)}) copy-start(f32[2048]{0:T(1024)} %param.26) | copy-start | bytes 24580
  202.8 144.7 %all-gather.16.cloned.1.call-start = ((), (), s32[]{:S(2)}) async-start(), calls=%async_computation.6 | async-start | bytes 6488064 | tf_op jit(solution)/shard_map/all_gather | solution.py:120
  203.3 236.9 %all-gather.18.cloned.1.call-start = ((), (), s32[]{:S(2)}) async-start(), calls=%async_computation.7 | async-start | bytes 6488064 | tf_op jit(solution)/shard_map/all_gather | solution.py:121
  204.1 329.5 %all-gather.20.cloned.1.call-start = ((), (), s32[]{:S(2)}) async-start(), calls=%async_computation.8 | async-start | bytes 6488064 | tf_op jit(solution)/shard_map/all_gather | solution.py:125
  204.8 142.7 %copy-start.23 = (f32[2048]{0:T(1024)S(1)}, f32[2048]{0:T(1024)}, u32[]{:S(2)}) copy-start(f32[2048]{0:T(1024)} %param.27) | copy-start | bytes 24580
  204.8 371.6 %reduce-scatter.2.cloned.1.call-start = ((), (), s32[]{:S(2)}) async-start(), calls=%async_computation.9 | async-start | bytes 2621440 | tf_op jit(solution)/shard_map/reduce_scatter | solution.py:128
  347.5 186.1 %copy-start.2 = (bf16[512,2048]{1,0:T(8,128)(2,1)S(1)}, bf16[512,2048]{1,0:T(8,128)(2,1)}, u32[]{:S(2)}) copy-start(bf16[512,2048]{1,0:T(8,128)(2,1)} %get-tuple-element.6) | copy-start | bytes 6291460
Sparse Core Ops, SparseCore 0:
  8.9 25.2 all-gather.7
  36.3 40.2 all-gather.9
  78.8 38.9 all-gather.11
  119.7 38.0 all-gather.13
  202.9 50.1 all-reduce.38
  255.1 92.3 all-gather.15
  349.7 90.4 all-gather.17
  442.2 91.2 all-gather.19
  547.1 29.3 reduce-scatter.1
where the time goes:
time: 595 us; the launch traced here: 592 us
  waiting for transfers between devices  409 us (69%)
  local copies, waits for them, and re-layouts  84 us (14%)
  other arithmetic  43.5 us (7%)
  matrix products  34.6 us (6%)
  between operations  14.2 us (2%)
    all_gather x1, waiting for transfers between devices, on_device(): lax.all_gather(hidden_down, 'fs', axis=1, tiled=True)  93.4 us
    all_gather x1, waiting for transfers between devices, on_device(): lax.all_gather(hidden_gate, 'fs', axis=0, tiled=True)  88.3 us
    all_gather x1, waiting for transfers between devices, on_device(): up_total = add_channel(lax.all_gather(hidden_up, 'fs', axis=0, tiled=True))  84.2 us
    slice x112, local copies, waits for them, and re-layouts, linear_scan(): lax.associative_scan(combine, (decay, inflow), axis=0, reverse=reverse)[1]  66.9 us
    psum x1, waiting for transfers between devices, on_device(): lax.psum(branch_part.astype(jnp.bfloat16), 'tp').astype(jnp.float32)  47.9 us
    all_gather x1, waiting for transfers between devices, on_device(): recur_total = add_mixer(lax.all_gather(recur_in, 'fs', axis=0, tiled=True))  40.3 us
    reduce_scatter x1, waiting for transfers between devices, on_device(): lax.psum_scatter(hidden_part.astype(jnp.bfloat16), 'tp', scatter_dimensio...  28.7 us
    all_gather x1, waiting for transfers between devices, on_device(): gathered_in = lax.all_gather(tokens, 'tp', axis=1, tiled=True)  21.9 us
  transfers between devices with their start and end apart: 9, of which 7 were waited for; matrix products, arithmetic and copies ran while one was open for 24% of the time, Pallas kernels for 0%

commit v1 on v0

--- a/solution.py
+++ b/solution.py
@@ -109,7 +109,9 @@
         lax.all_gather(recur_out, "fs", axis=1, tiled=True),
         preferred_element_type=jnp.float32,
     )
-    branch_sum = lax.psum(branch_part.astype(jnp.bfloat16), "tp").astype(jnp.float32)
+    branch_sum = jnp.sum(lax.all_gather(branch_part.astype(jnp.bfloat16), "tp"), axis=0).astype(
+        jnp.float32
+    )
     mid_full = (gathered_float + rms_scale(branch_sum, mixer_post)).astype(jnp.bfloat16)
     mid_own = lax.dynamic_slice_in_dim(mid_full, feature_start, feature_width, 1)
     channel_in = rms_scale(mid_full.astype(jnp.float32), channel_gain).astype(jnp.bfloat16)

time: 595 us -> 561 us (0.943)
  local copies, waits for them, and re-layouts: 84 us -> 39.5 us
  waiting for transfers between devices: 409 us -> 435 us
  other arithmetic: 43.5 us -> 30.7 us
    all_gather x0 -> x1, waiting for transfers between devices: none -> 55.1 us  [on_device(): lax.all_gather(branch_part.astype(jnp.bfloat16), 'tp')]
    psum x1 -> x0, waiting for transfers between devices: 47.9 us -> none  [on_device(): lax.psum(branch_part.astype(jnp.bfloat16), 'tp').astype(jnp.float32)]
    slice x112, local copies, waits for them, and re-layouts: 66.9 us -> 24.9 us  [linear_scan(): lax.associative_scan(combine, (decay, inflow), axis=0, reverse=reverse)[1]]
    all_gather x1, waiting for transfers between devices: 0.02 us -> 22.2 us  [on_device(): lax.all_gather(recur_out, 'fs', axis=1, tiled=True)]
    mul x14, other arithmetic: 10.6 us -> 1.28 us  [combine(): return (former[0] * latter[0], latter[0] * former[1] + latter[1])]
  transfers between devices with their start and end apart: 9 -> 9, of which waited for: 7 -> 8; matrix products, arithmetic and copies ran while one was open for 24% -> 15% of each run, Pallas kernels for 0% -> 0%
where the time goes in v1:
time: 561 us; the launch traced here: 560 us
  waiting for transfers between devices  435 us (78%)
  local copies, waits for them, and re-layouts  39.5 us (7%)
  matrix products  34.6 us (6%)
  other arithmetic  30.7 us (5%)
  between operations  14.3 us (3%)
  blocking collectives  5.76 us (1%)
    all_gather x1, waiting for transfers between devices, on_device(): lax.all_gather(hidden_down, 'fs', axis=1, tiled=True)  93.4 us
    all_gather x1, waiting for transfers between devices, on_device(): up_total = add_channel(lax.all_gather(hidden_up, 'fs', axis=0, tiled=True))  84.3 us
    all_gather x1, waiting for transfers between devices, on_device(): lax.all_gather(hidden_gate, 'fs', axis=0, tiled=True)  84.1 us
    all_gather x1, waiting for transfers between devices, on_device(): lax.all_gather(branch_part.astype(jnp.bfloat16), 'tp')  55.1 us
    all_gather x1, waiting for transfers between devices, on_device(): recur_total = add_mixer(lax.all_gather(recur_in, 'fs', axis=0, tiled=True))  40.3 us
    reduce_scatter x1, waiting for transfers between devices, on_device(): lax.psum_scatter(hidden_part.astype(jnp.bfloat16), 'tp', scatter_dimensio...  28.7 us
    slice x112, local copies, waits for them, and re-layouts, linear_scan(): lax.associative_scan(combine, (decay, inflow), axis=0, reverse=reverse)[1]  24.9 us
    all_gather x1, waiting for transfers between devices, on_device(): lax.all_gather(recur_out, 'fs', axis=1, tiled=True)  22.2 us
  transfers between devices with their start and end apart: 9, of which 8 were waited for; matrix products, arithmetic and copies ran while one was open for 15% of the time, Pallas kernels for 0%

profile of v1, /device:TPU:0, one launch (start us, length us, event | category | flops | bytes accessed | tf_op | source)
XLA Modules:
  0.0 560.1 jit_solution(11063026870556124738)
XLA Ops:
  6.5 0.7 all-gather.10.cloned.1.call-update
  7.3 0.7 all-gather.12.cloned.1.call-update
  8.1 0.7 all-gather.14.cloned.1.call-update
  9.4 0.7 dynamic-slice_convert_fusion
  10.1 1.3 dynamic_slice.25
  11.4 0.8 fusion.85
  12.3 21.9 %all-gather.10.cloned.1.call-done = bf16[512,2048]{1,0:T(8,128)(2,1)} async-done(((bf16[512,512]{1,0:T(8,128)(2,1)}), bf16[512,2048]{1,0:T(8,128)(2,1)}) %all-gather.10.cloned.1.call-update) | async-done | bytes 2097168 | tf_op jit(solution)/shard_map/all_gather | solution.py:85
  34.2 2.1 fusion.5
  36.3 40.3 %all-gather.12.cloned.1.call-done = bf16[2048,256]{1,0:T(8,128)(2,1)} async-done(((bf16[256,256]{1,0:T(8,128)(2,1)}), bf16[2048,256]{1,0:T(8,128)(2,1)}) %all-gather.12.cloned.1.call-update) | async-done | bytes 1048592 | tf_op jit(solution)/shard_map/all_gather | solution.py:92
  76.6 2.6 fusion.22
  80.8 2.1 fusion.21
  82.9 1.3 fusion.17
  84.4 2.1 copy.33
  86.5 1.0 copy.29
  87.5 1.0 copy.31
  88.5 2.3 multiply_exponential_fusion
  92.1 1.4 slice.489
  93.5 1.0 fusion.95
  96.7 0.6 slice.520
  97.3 0.6 slice.537
  98.4 0.6 slice.514
  99.0 0.6 slice.539
  100.2 0.6 slice.541
  101.4 0.6 slice.502
  102.0 0.6 slice.543
  102.6 0.6 slice.633
  103.3 0.6 slice.632
  110.2 1.4 slice.554
  111.6 1.4 slice.624
  112.9 0.6 slice.660
  113.5 0.6 pad_maximum_fusion.14
  114.2 0.7 pad.118
  114.9 0.7 fusion.75
  115.5 0.6 pad_maximum_fusion.12
  116.2 0.7 fusion.73
  116.9 0.7 pad_maximum_fusion.10
  117.6 0.7 fusion.71
  118.3 0.6 pad_maximum_fusion.8
  119.0 0.8 fusion.69
  119.8 0.7 pad_maximum_fusion.6
  120.9 1.7 pad.132
  122.6 1.7 pad.131
  125.1 2.0 slice.555
  127.1 3.1 slice.625
  130.2 1.0 fusion.57
  131.3 0.9 add.407
  132.2 3.4 rev.2
  135.7 22.2 %all-gather.16.cloned.1.call-done = bf16[256,2048]{1,0:T(8,128)(2,1)} async-done(((bf16[256,256]{1,0:T(8,128)(2,1)}), bf16[256,2048]{1,0:T(8,128)(2,1)}) %all-gather.16.cloned.1.call-update) | async-done | bytes 1048592 | tf_op jit(solution)/shard_map/all_gather | solution.py:109
  157.9 5.8 %convolution_convert_fusion = bf16[512,2048]{1,0:T(8,128)(2,1)} fusion(bf16[256,2048]{1,0:T(8,128)(2,1)} %all-gather.16.cloned.1.call-done, bf16[2048,256]{1,0:T(8,128)(2,1)} %all-gather.14.cloned.1.call-done, bf16[512,2048]{1,0:T(8,128)(2,1)S(1)} %copy-done.2, f32[2048]{0:T(1024)S(1)} %copy-done.12, f32[512]{0:T(512)S(1)} %copy-done.10, ...), kind=kOutput, calls=%fused_computation.17 | convolution fusion | flops 1080950784 | bytes 7875584 | tf_op jit(solution)/shard_map/dot_general | solution.py:107
  164.3 0.7 all-gather.20.cloned.1.call-update
  165.0 0.7 all-gather.22.cloned.1.call-update
  166.0 55.1 %all-gather.24.cloned.1.call-done = bf16[2048,2048]{1,0:T(8,128)(2,1)} async-done(((bf16[512,2048]{1,0:T(8,128)(2,1)}), bf16[2048,2048]{1,0:T(8,128)(2,1)}) %all-gather.24.cloned.1.call-update) | async-done | bytes 8388624 | tf_op jit(solution)/shard_map/all_gather | solution.py:112
  221.1 5.7 %reduce_sum.49 = bf16[512,2048]{1,0:T(8,128)(2,1)S(1)} reduce(bf16[4,512,2048]{2,1,0:T(8,128)(2,1)} %bitcast.46, bf16[]{:T(256)} %constant.47.clone.1), dimensions={0}, to_apply=%region_1.2 | reduce | flops 3145728 | bytes 10485762 | tf_op jit(solution)/shard_map/reduce_sum | solution.py:112
  227.3 4.1 fusion.2
  231.3 84.1 %all-gather.18.cloned.1.call-done = bf16[2048,1408]{1,0:T(8,128)(2,1)} async-done(((bf16[256,1408]{1,0:T(8,128)(2,1)}), bf16[2048,1408]{1,0:T(8,128)(2,1)}) %all-gather.18.cloned.1.call-update) | async-done | bytes 5767184 | tf_op jit(solution)/shard_map/all_gather | solution.py:122
  315.5 8.4 %fusion.30 = f32[512,1408]{1,0:T(8,128)} fusion(bf16[2048,1408]{1,0:T(8,128)(2,1)} %all-gather.18.cloned.1.call-done, bf16[512,2048]{1,0:T(8,128)(2,1)} %get-tuple-element.6, f32[2048]{0:T(1024)S(1)} %copy-done.13, f32[512]{0:T(512)S(1)} %add_rsqrt_fusion.1), kind=kOutput, calls=%fused_computation.47 | convolution fusion | flops 2956984320 | bytes 10758144 | tf_op jit(solution)/shard_map/dot_general | solution.py:58
  323.9 84.3 %all-gather.20.cloned.1.call-done = bf16[2048,1408]{1,0:T(8,128)(2,1)} async-done(((bf16[256,1408]{1,0:T(8,128)(2,1)}), bf16[2048,1408]{1,0:T(8,128)(2,1)}) %all-gather.20.cloned.1.call-update) | async-done | bytes 5767184 | tf_op jit(solution)/shard_map/all_gather | solution.py:123
  408.2 93.4 %all-gather.22.cloned.1.call-done = bf16[1408,2048]{1,0:T(8,128)(2,1)} async-done(((bf16[1408,256]{1,0:T(8,128)(2,1)}), bf16[1408,2048]{1,0:T(8,128)(2,1)}) %all-gather.22.cloned.1.call-update) | async-done | bytes 5767184 | tf_op jit(solution)/shard_map/all_gather | solution.py:127
  501.5 13.4 %convolution_convert_fusion.1 = bf16[512,2048]{1,0:T(8,128)(2,1)} fusion(bf16[1408,2048]{1,0:T(8,128)(2,1)} %all-gather.22.cloned.1.call-done, bf16[2048,1408]{1,0:T(8,128)(2,1)} %all-gather.20.cloned.1.call-done, f32[512,1408]{1,0:T(8,128)} %fusion.30, bf16[512,2048]{1,0:T(8,128)(2,1)S(1)} %copy-done.3, f32[2048]{0:T(1024)S(1)} %copy-done.13, ...), kind=kOutput, calls=%fused_computation.19 | convolution fusion | flops 5915148288 | bytes 18622464 | tf_op jit(solution)/shard_map/dot_general | solution.py:125
  515.0 0.8 dynamic_slice.27
  515.7 28.7 %reduce-scatter.2.cloned.1.call-done = bf16[512,512]{1,0:T(8,128)(2,1)} async-done(((bf16[512,2048]{1,0:T(8,128)(2,1)}), bf16[512,512]{1,0:T(8,128)(2,1)}) %reduce-scatter.2.cloned.1.call-update) | async-done | bytes 524304 | tf_op jit(solution)/shard_map/reduce_scatter | solution.py:130
  544.5 1.2 fusion.24
  545.7 5.8 %psum.7 = f32[512]{0:T(512)S(1)} all-reduce(f32[512]{0:T(512)S(1)} %fusion.24), channel_id=1, replica_groups=mesh['fs'=8,'tp'=4] {'tp'}, use_global_device_ids=true, to_apply=%region_6.7 | all-reduce | flops 512 | bytes 4096 | tf_op jit(solution)/shard_map/psum | solution.py:133
  551.5 2.1 fusion.27
  (234 shorter events, 16.0 us)
Async XLA Ops:
  6.5 73.2 %copy-start = (bf16[2,16,64,64]{3,2,1,0:T(8,128)(2,1)S(1)}, bf16[2,16,64,64]{3,2,1,0:T(8,128)(2,1)}, u32[]{:S(2)}) copy-start(bf16[2,16,64,64]{3,2,1,0:T(8,128)(2,1)} %param.22) | copy-start | bytes 786436
  6.5 27.7 %all-gather.10.cloned.1.call-start = ((), (), s32[]{:S(2)}) async-start(), calls=%async_computation.1 | async-start | bytes 2621440 | tf_op jit(solution)/shard_map/all_gather | solution.py:85
  7.3 69.4 %all-gather.12.cloned.1.call-start = ((), (), s32[]{:S(2)}) async-start(), calls=%async_computation.2 | async-start | bytes 1179648 | tf_op jit(solution)/shard_map/all_gather | solution.py:92
  8.0 127.6 %all-gather.14.cloned.1.call-start = ((), (), s32[]{:S(2)}) async-start(), calls=%async_computation.3 | async-start | bytes 1179648 | tf_op jit(solution)/shard_map/all_gather | solution.py:93
  8.7 149.1 %all-gather.16.cloned.1.call-start = ((), (), s32[]{:S(2)}) async-start(), calls=%async_computation.4 | async-start | bytes 1179648 | tf_op jit(solution)/shard_map/all_gather | solution.py:109
  9.3 211.7 %all-gather.24.cloned.1.call-start = ((), (), s32[]{:S(2)}) async-start(), calls=%async_computation.9 | async-start | bytes 10485760 | tf_op jit(solution)/shard_map/all_gather | solution.py:112
  36.3 43.9 %copy-start.9 = (f32[512]{0:T(512)}, f32[512]{0:T(512)S(1)}, u32[]{:S(2)}) copy-start(f32[512]{0:T(512)S(1)} %add_rsqrt_fusion.3) | copy-start | bytes 6148
  108.2 12.3 %copy-start.7 = (f32[1,256]{1,0:T(1,128)S(1)}, f32[1,256]{1,0:T(1,128)}, u32[]{:S(2)}) copy-start(f32[1,256]{1,0:T(1,128)} %slice.632) | copy-start | bytes 3076
  108.5 12.2 %copy-start.6 = (f32[1,256]{1,0:T(1,128)S(1)}, f32[1,256]{1,0:T(1,128)}, u32[]{:S(2)}) copy-start(f32[1,256]{1,0:T(1,128)} %slice.631) | copy-start | bytes 3076
  109.9 12.7 %copy-start.5 = (f32[1,256]{1,0:T(1,128)S(1)}, f32[1,256]{1,0:T(1,128)}, u32[]{:S(2)}) copy-start(f32[1,256]{1,0:T(1,128)} %slice.630) | copy-start | bytes 3076
  124.3 6.9 %copy-start.8 = (f32[1,256]{1,0:T(1,128)S(1)}, f32[1,256]{1,0:T(1,128)}, u32[]{:S(2)}) copy-start(f32[1,256]{1,0:T(1,128)} %slice.660) | copy-start | bytes 3076
  124.9 32.9 %copy-start.2 = (bf16[512,2048]{1,0:T(8,128)(2,1)S(1)}, bf16[512,2048]{1,0:T(8,128)(2,1)}, u32[]{:S(2)}) copy-start(bf16[512,2048]{1,0:T(8,128)(2,1)} %all-gather.10.cloned.1.call-done) | copy-start | bytes 6291460
  124.9 32.9 %copy-start.10 = (f32[512]{0:T(512)S(1)}, f32[512]{0:T(512)}, u32[]{:S(2)}) copy-start(f32[512]{0:T(512)} %copy-done.9) | copy-start | bytes 6148
  125.0 32.9 %copy-start.11 = (f32[256]{0:T(256)S(1)}, f32[256]{0:T(256)}, u32[]{:S(2)}) copy-start(f32[256]{0:T(256)} %dynamic_slice.25) | copy-start | bytes 3076
  125.0 32.9 %copy-start.12 = (f32[2048]{0:T(1024)S(1)}, f32[2048]{0:T(1024)}, u32[]{:S(2)}) copy-start(f32[2048]{0:T(1024)} %param.17) | copy-start | bytes 24580
  163.6 151.8 %all-gather.18.cloned.1.call-start = ((), (), s32[]{:S(2)}) async-start(), calls=%async_computation.5 | async-start | bytes 6488064 | tf_op jit(solution)/shard_map/all_gather | solution.py:122
  164.2 243.9 %all-gather.20.cloned.1.call-start = ((), (), s32[]{:S(2)}) async-start(), calls=%async_computation.6 | async-start | bytes 6488064 | tf_op jit(solution)/shard_map/all_gather | solution.py:123
  165.0 336.6 %all-gather.22.cloned.1.call-start = ((), (), s32[]{:S(2)}) async-start(), calls=%async_computation.7 | async-start | bytes 6488064 | tf_op jit(solution)/shard_map/all_gather | solution.py:127
  165.7 378.8 %reduce-scatter.2.cloned.1.call-start = ((), (), s32[]{:S(2)}) async-start(), calls=%async_computation.8 | async-start | bytes 2621440 | tf_op jit(solution)/shard_map/reduce_scatter | solution.py:130
  221.1 6.2 %copy-start.4 = (f32[2048]{0:T(1024)S(1)}, f32[2048]{0:T(1024)}, u32[]{:S(2)}) copy-start(f32[2048]{0:T(1024)} %param.26) | copy-start | bytes 24580
  226.8 88.7 %copy-start.13 = (f32[2048]{0:T(1024)S(1)}, f32[2048]{0:T(1024)}, u32[]{:S(2)}) copy-start(f32[2048]{0:T(1024)} %param.27) | copy-start | bytes 24580
  315.5 186.1 %copy-start.3 = (bf16[512,2048]{1,0:T(8,128)(2,1)S(1)}, bf16[512,2048]{1,0:T(8,128)(2,1)}, u32[]{:S(2)}) copy-start(bf16[512,2048]{1,0:T(8,128)(2,1)} %get-tuple-element.6) | copy-start | bytes 6291460
  501.5 52.0 %copy-start.1 = (bf16[2,16,64,64]{3,2,1,0:T(8,128)(2,1)S(1)}, bf16[2,16,64,64]{3,2,1,0:T(8,128)(2,1)}, u32[]{:S(2)}) copy-start(bf16[2,16,64,64]{3,2,1,0:T(8,128)(2,1)} %param.22) | copy-start | bytes 786436
Sparse Core Ops, SparseCore 0:
  8.9 25.2 all-gather.9
  36.3 40.2 all-gather.11
  78.8 38.9 all-gather.13
  119.7 38.0 all-gather.15
  163.8 57.2 all-gather.23
  223.1 92.3 all-gather.17
  317.6 90.4 all-gather.19
  410.2 91.2 all-gather.21
  515.1 29.3 reduce-scatter.1
